TPU v7x, 32 devices: a whole 2x2x4 slice. The times are simulated.
32 devices in a mesh: ep: 8 (over z, y), tp: 4 (over x, core).
Axes of the slice: x: 2, y: 2, z: 4, core: 2. Of those that a mesh axis runs over, the one named last changes fastest.
Arguments:
- tokens: bfloat16 [2048, 2048], P('ep', 'tp'), may hold values from -400 to 400
- expert_ids: int32 [2048, 2], P('ep'), may hold values from 0 to 7, all different within a row; in each aligned block of 256 rows (0 to 255, 256 to 511, ...) at most 80 rows name the same one
- route_weights: float32 [2048, 2], P('ep'), may hold values from 0.1 to 1
- pre_gain: float32 [2048], P('tp'), may hold values from 0.1 to 1.9
- post_gain: float32 [2048], P('tp'), may hold values from 0.1 to 1.9
- gate_weight: bfloat16 [8, 2048, 4096], P('ep', None, 'tp'), may hold values from -0.125 to 0.125
- up_weight: bfloat16 [8, 2048, 4096], P('ep', None, 'tp'), may hold values from -0.125 to 0.125
- down_weight: bfloat16 [8, 4096, 2048], P('ep', None, 'tp'), may hold values from -0.71875 to 0.71875
Outputs:
- layer_out: bfloat16 [2048, 2048], P('ep', 'tp')
Inputs may be any that keep to these rules, and one draw needn't show every extreme that they name: `expert_ids`: the 2 experts of a token are distinct. Within the rows of one device along ep, no expert is named more than 80 times, a bound that some block reaches.
All inputs are finite; a program needn't handle non-finite values.
Results may differ from a plain program's by a relative error of at most 0.007.
Values may be sent and summed in bfloat16 or wider, within the bound.
A program may use at most 64 MiB of HBM per device.

v0:
```python
import functools

import jax
import jax.numpy as jnp
from jax import lax
from jax.experimental import pallas as pl
from jax.experimental.pallas import tpu as pltpu
from jax.sharding import PartitionSpec as P

epsilon = 1e-06
MESH = pl.DeviceIdType.MESH
f32, bf16 = jnp.float32, jnp.bfloat16


def flip(index, bits):
    out, bit = index, 1
    while bit <= bits:
        if bits & bit:
            out = out + bit * (1 - 2 * ((index // bit) % 2))
        bit *= 2
    return out


def to_column(row):
    return jnp.transpose(jnp.broadcast_to(row, (128, row.shape[1])))


def wide(column, width):
    return jnp.concatenate([column] * (width // 128), axis=1)


def row_sums(values):
    part = values[:, 0:128]
    for at in range(128, values.shape[1], 128):
        part = part + values[:, at : at + 128]
    return jnp.sum(jnp.transpose(part), axis=0, keepdims=True)


def kernel(
    n, tp, cap, groups, chunks, pieces,
    tok_ref, ids_ref, rw_ref, pre_ref, post_ref, wg_hbm, wu_hbm, wd_hbm,
    out_ref,
    wg, wu, wd, outg, feats, rows_in, hid, back, ret, gain, ss_out, mix, wcol, *rest,
):
    picks, sems = rest[: len(pieces)], rest[len(pieces) :]
    (w_sem, g_s, g_r, so_s, so_r, d_s, d_r, fx_s, fx_r, fp_s, fp_r,
     hx_s, hx_r, hp_s, hp_r, r_s, r_r) = sems
    me, ti = lax.axis_index("ep"), lax.axis_index("tp")
    chips = tp // 2
    chip, core = ti // 2, ti % 2
    partner = chip * 2 + (1 - core)
    rows, width = tok_ref.shape
    units = wg.shape[1]
    n_tile = min(256, units)
    tiles = units // n_tile
    per_group = n // groups
    group_rows = per_group * cap

    barrier = pltpu.get_barrier_semaphore()
    for d in range(1, n):
        pl.semaphore_signal(barrier, inc=1, device_id={"ep": flip(me, d)}, device_id_type=MESH)
    for j in range(1, tp):
        pl.semaphore_signal(barrier, inc=1, device_id={"tp": (ti + j) % tp}, device_id_type=MESH)
    loads = [
        pltpu.make_async_copy(src.at[0], dst, w_sem.at[i])
        for i, (src, dst) in enumerate(((wg_hbm, wg), (wu_hbm, wu), (wd_hbm, wd)))
    ]
    for load in loads:
        load.start()

    def remote(src, dst, s_sem, r_sem, where):
        return pltpu.make_async_remote_copy(
            src_ref=src, dst_ref=dst, send_sem=s_sem, recv_sem=r_sem,
            device_id=where, device_id_type=MESH,
        )

    def go(copy):
        copy.start()

    lanes = max(n, 16)
    rel = [jnp.bitwise_xor(ids_ref[k : k + 1, :], me) for k in range(2)]
    d_iota = lax.broadcasted_iota(jnp.int32, (lanes, rows), 0)
    hot = [jnp.where(rel[k] == d_iota, 1.0, 0.0).astype(f32) for k in range(2)]
    earlier = jnp.where(
        lax.broadcasted_iota(jnp.int32, (rows, rows), 0)
        < lax.broadcasted_iota(jnp.int32, (rows, rows), 1), 1.0, 0.0,
    ).astype(bf16)
    prefix = jnp.dot((hot[0] + hot[1]).astype(bf16), earlier, preferred_element_type=f32)
    target = [
        rel[k].astype(f32) * cap + jnp.sum(prefix * hot[k], axis=0, keepdims=True)
        for k in range(2)
    ]
    slot_iota = lax.broadcasted_iota(jnp.int32, (cap, rows), 0).astype(f32)

    tokens = tok_ref[...]
    own = pl.ds(pl.multiple_of(ti * width, 128), width)

    def block(d):
        return pl.ds(d * cap, cap)

    def group(g):
        return pl.ds(g * group_rows, group_rows)

    def dispatch_copy(d):
        return remote(
            outg.at[block(d)], feats.at[block(d), own], d_s.at[0], d_r.at[d - 1], {"ep": flip(me, d)}
        )

    def feat_x(g, j):
        ref = feats.at[group(g), own]
        where = {"tp": ((chip + j) % chips) * 2 + core}
        return remote(ref, ref, fx_s.at[0], fx_r.at[g, j - 1], where)

    def feat_pair(g, j):
        source = ((chip + chips - j) % chips) * 2 + core
        ref = feats.at[group(g), pl.ds(pl.multiple_of(source * width, 128), width)]
        return remote(ref, ref, fp_s.at[0], fp_r.at[g], {"tp": partner})

    def share(g):
        for j in range(1, chips):
            go(feat_x(g, j))
        go(feat_pair(g, 0))

    def pass_on(g):
        for j in range(1, chips):
            feat_x(g, j).wait_recv()
            go(feat_pair(g, j))

    for d in range(n):
        base = float(d * cap)
        chosen = jnp.where(
            (target[0] == slot_iota + base) | (target[1] == slot_iota + base), 1.0, 0.0
        ).astype(bf16)
        picked = jnp.dot(chosen, tokens, preferred_element_type=f32).astype(bf16)
        if d == 0:
            feats[block(0), own] = picked
        else:
            outg[block(d), :] = picked
    pl.semaphore_wait(barrier, n - 1 + tp - 1)
    if per_group == 1:
        share(0)
    for d in range(1, n):
        go(dispatch_copy(d))
    gain[:, own] = pre_ref[...]

    def gain_copy(j):
        return remote(pre_ref, gain.at[:, own], g_s.at[0], g_r.at[j - 1], {"tp": (ti + j) % tp})

    for j in range(1, tp):
        go(gain_copy(j))

    def piece_slots(piece):
        return pl.ds(piece[0] * group_rows, piece[1] * group_rows)

    for k in range(2):
        column = to_column(target[k])
        wcol[k] = to_column(rw_ref[k : k + 1, :])
        for piece, pick in zip(pieces, picks):
            base = piece[0] * group_rows
            for at in range(0, pick.shape[2], 128):
                size = min(128, pick.shape[2] - at)
                lane = lax.broadcasted_iota(jnp.int32, (rows, size), 1).astype(f32)
                pick[k, :, at : at + size] = jnp.where(
                    column[:, 0:size] == lane + float(base + at), 1.0, 0.0
                ).astype(bf16)

    def combine(piece, pick, first):
        value = 0.0 if first else mix[...]
        for k in range(2):
            found = jnp.dot(pick[k], ret[piece_slots(piece), :], preferred_element_type=f32)
            value = value + found * wide(wcol[k], width)
        return value

    def chunk(q):
        return pl.ds(chunks[q][0] * group_rows, chunks[q][1] * group_rows)

    def hid_ref(q, owner, i):
        at = pl.multiple_of(owner * units + i * n_tile, 128)
        return hid.at[chunk(q), pl.ds(at, n_tile)]

    def hid_x(q, i, j):
        ref = hid_ref(q, ti, i)
        where = {"tp": ((chip + j) % chips) * 2 + core}
        return remote(ref, ref, hx_s.at[0], hx_r.at[q, i, j - 1], where)

    def hid_pair(q, i, j):
        ref = hid_ref(q, ((chip + chips - j) % chips) * 2 + core, i)
        return remote(ref, ref, hp_s.at[0], hp_r.at[q], {"tp": partner})

    def send_tile(q, i):
        for j in range(1, chips):
            hid_x(q, i, j).start()
        hid_pair(q, i, 0).start()

    def send_hidden(q):
        def body(i, carry):
            send_tile(q, i)
            return carry

        lax.fori_loop(0, tiles, body, 0)

    def gate_up(first, many, q=None):
        for g in range(first, first + many):
            ref = feats.at[group(g), 0 : chips * width]
            remote(ref, ref, fp_s.at[0], fp_r.at[g], {"tp": partner}).wait_recv()

        at, count = first * group_rows, many * group_rows
        span = pl.ds(at, count)
        batch = max(u for u in range(1, 6) if (count // 16) % u == 0)

        def norm(i, carry):
            for u in range(batch):
                here = (i * batch + u) * 16
                part = pl.ds(pl.multiple_of(at + here, 16), 16)
                x = feats[part, :].astype(f32)
                square = jnp.sum(x * x, axis=1, keepdims=True)
                x = x * lax.rsqrt(square / (width * tp) + epsilon) * gain[...]
                rows_in[pl.ds(pl.multiple_of(here, 16), 16), :] = x.astype(bf16)
            return carry

        lax.fori_loop(0, count // (16 * batch), norm, 0)

        def tile(i, carry):
            cols = pl.ds(pl.multiple_of(i * n_tile, 128), n_tile)
            x = rows_in[0:count, :]
            gate = jnp.dot(x, wg[:, cols], preferred_element_type=f32)
            upper = jnp.dot(x, wu[:, cols], preferred_element_type=f32)
            value = gate / (1.0 + jnp.exp(-gate)) * upper
            mine = pl.ds(pl.multiple_of(ti * units + i * n_tile, 128), n_tile)
            hid[span, mine] = value.astype(bf16)
            if q is not None:
                send_tile(q, i)
            return carry

        lax.fori_loop(0, tiles, tile, 0)

    def take(g):
        for d in range(g * per_group, (g + 1) * per_group):
            if d > 0:
                dispatch_copy(d).wait_recv()
        if not (g == 0 and per_group == 1):
            share(g)

    out_tile = min(256, width)

    def return_copy(d):
        return remote(back.at[block(d)], ret.at[block(d)], r_s.at[0], r_r.at[d - 1], {"ep": flip(me, d)})

    def finish(q):
        def relay(i, carry):
            for j in range(1, chips):
                hid_x(q, i, j).wait_recv()
                hid_pair(q, i, j).start()
            return carry

        lax.fori_loop(0, tiles, relay, 0)
        ref = hid.at[chunk(q), 0 : chips * units]
        remote(ref, ref, hp_s.at[0], hp_r.at[q], {"tp": partner}).wait_recv()

        def down(i, carry):
            cols = pl.ds(pl.multiple_of(i * out_tile, 128), out_tile)
            back[chunk(q), cols] = jnp.dot(
                hid[chunk(q), :], wd[:, cols], preferred_element_type=f32
            ).astype(bf16)
            return carry

        lax.fori_loop(0, width // out_tile, down, 0)
        for d in range(chunks[q][0] * per_group, sum(chunks[q]) * per_group):
            if d > 0:
                go(return_copy(d))
        if chunks[q][0] == 0:
            ret[block(0), :] = back[block(0), :]

    take(0)
    for g in range(1, 6):
        take(g)
        if g > 1:
            pass_on(g - 2)
    loads[0].wait()
    loads[1].wait()
    for j in range(1, tp):
        gain_copy(j).wait_recv()
    gate_up(2, 2, 0)
    pass_on(4)
    take(6)
    take(7)
    pass_on(5)
    gate_up(4, 2, 1)
    gate_up(0, 2)
    loads[2].wait()
    finish(0)
    pass_on(6)
    pass_on(7)
    gate_up(6, 2, 2)
    send_hidden(3)
    send_hidden(4)
    finish(1)
    finish(2)
    finish(3)
    piece = pieces[0]
    for d in range(piece[0] * per_group, sum(piece) * per_group):
        return_copy(d).wait_recv()
    mix[...] = combine(piece, picks[0], True)
    finish(4)
    for piece, pick in zip(pieces[1:], picks[1:]):
        for d in range(piece[0] * per_group, sum(piece) * per_group):
            if d > 0:
                return_copy(d).wait_recv()
        mix[...] = combine(piece, pick, False)
    mixed = mix[...]
    ss_out[0] = row_sums(mixed * mixed)
    out_copies = [
        remote(ss_out.at[0], ss_out.at[j], so_s.at[0], so_r.at[j - 1], {"tp": (ti + j) % tp})
        for j in range(1, tp)
    ]
    for copy in out_copies:
        copy.start()
    def drain(ref, sem):
        remote(ref, ref, sem.at[0], so_r.at[0], {"tp": partner}).wait_send()

    later = pl.ds(cap, (n - 1) * cap)
    drain(outg.at[later], d_s)
    drain(back.at[later], r_s)
    drain(gain.at[:, 0 : (tp - 1) * width], g_s)
    drain(feats.at[:, 0 : (chips - 1) * width], fx_s)
    drain(feats.at[:, 0 : chips * width], fp_s)
    drain(hid.at[:, 0 : (chips - 1) * units], hx_s)
    drain(hid.at[:, 0 : chips * units], hp_s)
    for copy in out_copies:
        copy.wait_recv()
    total = ss_out[0]
    for j in range(1, tp):
        total = total + ss_out[j]
    scale = wide(to_column(lax.rsqrt(total / (width * tp) + epsilon)), width)
    out_ref[...] = (mixed * scale * post_ref[...]).astype(bf16)
    drain(ss_out.at[0 : tp - 1], so_s)


def on_device(
    tokens, expert_ids, route_weights, pre_gain, post_gain, gate_weight, up_weight, down_weight
):
    rows, width = tokens.shape
    n, tp = lax.axis_size("ep"), lax.axis_size("tp")
    assert gate_weight.shape[0] == 1 and expert_ids.shape[1] == 2
    capacity = max(2, rows * 2 * 5 // (4 * n))
    cap = -(-capacity // 16) * 16
    groups = 8
    assert n % groups == 0
    chunks = ((2, 2), (4, 2), (6, 2), (1, 1), (0, 1))
    pieces = ((2, 4), (6, 2), (0, 2))
    slots = n * cap
    chips = tp // 2
    features, units = gate_weight.shape[1:]
    hidden_all = units * tp
    tiles = units // min(256, units)
    steps = len(chunks)
    most = max(count for _, count in chunks) * (slots // groups)
    dma = pltpu.SemaphoreType.DMA
    vmem = pl.BlockSpec(memory_space=pltpu.VMEM)
    hbm = pl.BlockSpec(memory_space=pl.ANY)
    return pl.pallas_call(
        functools.partial(kernel, n, tp, cap, groups, chunks, pieces),
        out_shape=jax.ShapeDtypeStruct((rows, width), bf16),
        in_specs=[vmem] * 5 + [hbm] * 3,
        out_specs=vmem,
        scratch_shapes=[
            pltpu.VMEM((features, units), bf16),
            pltpu.VMEM((features, units), bf16),
            pltpu.VMEM((hidden_all, width), bf16),
            pltpu.VMEM((slots, width), bf16),
            pltpu.VMEM((slots, features), bf16),
            pltpu.VMEM((most, features), bf16),
            pltpu.VMEM((slots, hidden_all), bf16),
            pltpu.VMEM((slots, width), bf16),
            pltpu.VMEM((slots, width), bf16),
            pltpu.VMEM((1, features), f32),
            pltpu.VMEM((tp, 1, rows), f32),
            pltpu.VMEM((rows, width), f32),
            pltpu.VMEM((2, rows, 128), f32),
            *[pltpu.VMEM((2, rows, count * (slots // groups)), bf16) for _, count in pieces],
            dma((3,)),
            dma((1,)), dma((tp - 1,)), dma((1,)), dma((tp - 1,)),
            dma((1,)), dma((n - 1,)),
            dma((1,)), dma((groups, chips - 1)),
            dma((1,)), dma((groups,)),
            dma((1,)), dma((steps, tiles, chips - 1)),
            dma((1,)), dma((steps,)),
            dma((1,)), dma((n - 1,)),
        ],
        compiler_params=pltpu.CompilerParams(
            collective_id=0, has_side_effects=True, vmem_limit_bytes=56 * 1024 * 1024
        ),
    )(
        tokens, jnp.transpose(expert_ids), jnp.transpose(route_weights),
        pre_gain.reshape(1, -1), post_gain.reshape(1, -1),
        gate_weight, up_weight, down_weight,
    )


def solution(mesh):
    return jax.shard_map(
        on_device,
        mesh=mesh,
        in_specs=(
            P("ep", "tp"),
            P("ep", None),
            P("ep", None),
            P("tp"),
            P("tp"),
            P("ep", None, "tp"),
            P("ep", None, "tp"),
            P("ep", None, "tp"),
        ),
        out_specs=P("ep", "tp"),
        check_vma=False,
    )
```

profile of v0, /device:TPU:0, one launch (start us, length us, event | category | flops | bytes accessed | tf_op | source)
XLA Modules:
  0.0 64.3 jit_solution(11520661105375984002)
XLA Ops:
  0.0 62.7 %shard_map.82 = bf16[256,512]{1,0:T(8,128)(2,1)} custom-call(bf16[256,512]{1,0:T(8,128)(2,1)} %tok_ref.1, s32[2,256]{1,0:T(2,128)} %bitcast.4, f32[2,256]{1,0:T(2,128)} %bitcast.5, f32[1,512]{1,0:T(1,128)} %bitcast.6, f32[1,512]{1,0:T(1,128)} %bitcast.7, bf16[1,2048,1024]{2,1,0:T(8,128)(2,1)} %wg_hbm.1, bf16[1,2048,1024]{2,1,0:T(8,128)(2,1)} %wu_hbm.1, ...), custom_call_target="tpu_custom_call" | custom-call | tf_op jit(solution)/shard_map/pallas_call | solution.py:361
  62.7 1.7 %copy.10 = bf16[256,512]{1,0:T(8,128)(2,1)} copy(bf16[256,512]{1,0:T(8,128)(2,1)} %shard_map.82) | data formatting | bytes 524288
where the time goes:
time: 64.5 us; the launch traced here: 64.3 us
  Pallas kernels  62.7 us (97%)
  local copies, waits for them, and re-layouts  1.67 us (3%)
    pallas_call x1, Pallas kernels, on_device(): pl.pallas_call(functools.partial(kernel, n, tp, cap, groups, chunks, piec...  62.7 us
    unnamed x1, local copies, waits for them, and re-layouts  1.67 us

commit v1 on v0

v1 whole, which is shorter than its diff:
```python
import functools

import jax
import jax.numpy as jnp
from jax import lax
from jax.experimental import pallas as pl
from jax.experimental.pallas import tpu as pltpu
from jax.sharding import PartitionSpec as P

epsilon = 1e-06
MESH = pl.DeviceIdType.MESH
f32, bf16 = jnp.float32, jnp.bfloat16


def flip(index, bits):
    out, bit = index, 1
    while bit <= bits:
        if bits & bit:
            out = out + bit * (1 - 2 * ((index // bit) % 2))
        bit *= 2
    return out


def to_column(row):
    return jnp.transpose(jnp.broadcast_to(row, (128, row.shape[1])))


def wide(column, width):
    return jnp.concatenate([column] * (width // 128), axis=1)


def row_sums(values):
    part = values[:, 0:128]
    for at in range(128, values.shape[1], 128):
        part = part + values[:, at : at + 128]
    return jnp.sum(jnp.transpose(part), axis=0, keepdims=True)


def kernel(
    n, tp, cap, groups, shared, early, pieces,
    tok_ref, ids_ref, rw_ref, pre_ref, post_ref, wg_hbm, wu_hbm, wd_hbm,
    out_ref,
    wg, wu, wd, tok_x, outg, feats, rows_in, hid, part, back, ret, gain, ss_out, mix, wcol, *rest,
):
    picks, sems = rest[: len(pieces)], rest[len(pieces) :]
    (w_sem, met_ep, met_tp, t_s, t_r, g_s, g_r, so_s, so_r, d_s, d_r, fx_s, fx_r, fp_s, fp_r,
     hx_s, hx_r, hp_s, hp_r, r_s, r_r) = sems
    me, ti = lax.axis_index("ep"), lax.axis_index("tp")
    chips = tp // 2
    chip, core = ti // 2, ti % 2
    partner = chip * 2 + (1 - core)
    rows, width = tok_ref.shape
    side = chips * width
    units = wg.shape[1]
    n_tile = min(256, units)
    tiles = units // n_tile
    per_group = n // groups
    group_rows = per_group * cap

    barrier = pltpu.get_barrier_semaphore()

    def signal(sem, where):
        pl.semaphore_signal(sem, inc=1, device_id=where, device_id_type=MESH)

    for j in range(1, tp):
        peer = (ti + j) % tp
        pl.when(peer > ti)(functools.partial(signal, barrier, {"tp": peer}))
    for d in range(1, n):
        peer = flip(me, d)
        pl.when(peer > me)(functools.partial(signal, barrier, {"ep": peer}))

    def load_all(src, dst, sem, step, place):
        for at in range(0, dst.shape[0], step):
            pltpu.make_async_copy(
                src.at[0, pl.ds(at, step)], dst.at[pl.ds(place(at // step) * step, step)], sem
            ).start()

    def position(owner):
        return owner % 2 * chips + owner // 2

    load_all(wg_hbm, wg, w_sem.at[0], width, position)
    load_all(wu_hbm, wu, w_sem.at[1], width, position)
    load_all(
        wd_hbm, wd, w_sem.at[2], n_tile, lambda at: at % tiles * tp + position(at // tiles)
    )
    loads = [
        pltpu.make_async_copy(src.at[0], dst, w_sem.at[i])
        for i, (src, dst) in enumerate(((wg_hbm, wg), (wu_hbm, wu), (wd_hbm, wd)))
    ]

    pl.when(me + ti > 0)(lambda: pl.semaphore_wait(barrier, me + ti))
    for j in range(1, tp):
        peer = (ti + j) % tp
        pl.when(peer < ti)(functools.partial(signal, met_tp.at[tp - j - 1], {"tp": peer}))
    for d in range(1, n):
        peer = flip(me, d)
        pl.when(peer < me)(functools.partial(signal, met_ep.at[d - 1], {"ep": peer}))

    def meet_tp(j):
        pl.when((ti + j) % tp > ti)(lambda: pl.semaphore_wait(met_tp.at[j - 1], 1))

    def meet_ep(d):
        pl.when(flip(me, d) > me)(lambda: pl.semaphore_wait(met_ep.at[d - 1], 1))

    def remote(src, dst, s_sem, r_sem, where):
        return pltpu.make_async_remote_copy(
            src_ref=src, dst_ref=dst, send_sem=s_sem, recv_sem=r_sem,
            device_id=where, device_id_type=MESH,
        )

    lanes = max(n, 16)
    rel = [jnp.bitwise_xor(ids_ref[k : k + 1, :], me) for k in range(2)]
    d_iota = lax.broadcasted_iota(jnp.int32, (lanes, rows), 0)
    hot = [jnp.where(rel[k] == d_iota, 1.0, 0.0).astype(f32) for k in range(2)]
    earlier = jnp.where(
        lax.broadcasted_iota(jnp.int32, (rows, rows), 0)
        < lax.broadcasted_iota(jnp.int32, (rows, rows), 1), 1.0, 0.0,
    ).astype(bf16)
    prefix = jnp.dot((hot[0] + hot[1]).astype(bf16), earlier, preferred_element_type=f32)
    target = [
        rel[k].astype(f32) * cap + jnp.sum(prefix * hot[k], axis=0, keepdims=True)
        for k in range(2)
    ]
    slot_iota = lax.broadcasted_iota(jnp.int32, (cap, rows), 0).astype(f32)

    def hop(j):
        return (chip + j) % chips

    def seg(j):
        return pl.ds(pl.multiple_of(core * side + hop(j) * width, 128), width)

    def tok_seg(j):
        return pl.ds(pl.multiple_of(hop(j) * width, 128), width)

    own = seg(0)
    half = pl.ds(pl.multiple_of(core * side, 128), side)

    def block(d):
        return pl.ds(d * cap, cap)

    def group(g):
        return pl.ds(g * group_rows, group_rows)

    def members(g):
        return range(g * per_group, (g + 1) * per_group)

    def token_copy(j):
        return remote(
            tok_ref, tok_x.at[:, tok_seg(0)], t_s.at[0], t_r.at[j - 1], {"tp": hop(j) * 2 + core}
        )

    def gain_copy(j):
        return remote(pre_ref, gain.at[:, own], g_s.at[0], g_r.at[j - 1], {"tp": (ti + j) % tp})

    def dispatch_copy(d, j):
        return remote(
            outg.at[block(d), tok_seg(j)], feats.at[block(d), seg(j)],
            d_s.at[0], d_r.at[d - 1, j], {"ep": flip(me, d)},
        )

    def feat_x(g, j):
        ref = feats.at[group(g), own]
        return remote(ref, ref, fx_s.at[0], fx_r.at[g, j - 1], {"tp": hop(j) * 2 + core})

    def feat_pair(g):
        ref = feats.at[group(g), half]
        return remote(ref, ref, fp_s.at[0], fp_r.at[g], {"tp": partner})

    def choose(d, j):
        base = float(d * cap)
        chosen = jnp.where(
            (target[0] == slot_iota + base) | (target[1] == slot_iota + base), 1.0, 0.0
        ).astype(bf16)
        source = tok_ref[...] if j == 0 else tok_x[:, tok_seg(j)]
        picked = jnp.dot(chosen, source, preferred_element_type=f32).astype(bf16)
        if d == 0:
            feats[block(0), seg(j)] = picked
        else:
            outg[block(d), tok_seg(j)] = picked

    def pick_own(g):
        for d in members(g):
            choose(d, 0)

    def send_own(g):
        for d in members(g):
            if d > 0:
                meet_ep(d)
                dispatch_copy(d, 0).start()

    def send_rest(g):
        for d in members(g):
            for j in range(1, chips):
                choose(d, j)
                if d > 0:
                    dispatch_copy(d, j).start()

    def take(g):
        for d in members(g):
            for j in range(1 if g in shared else chips):
                if d > 0:
                    dispatch_copy(d, j).wait_recv()
        if g in shared:
            for j in range(1, chips):
                feat_x(g, j).start()
        else:
            feat_pair(g).start()

    def pass_on(g):
        for j in range(1, chips):
            feat_x(g, j).wait_recv()
        feat_pair(g).start()

    def tile_at(i, owner):
        return pl.multiple_of((i * tp + position(owner)) * n_tile, 128)

    def hid_x(g, i, j):
        ref = hid.at[group(g), pl.ds(tile_at(i, ti), n_tile)]
        return remote(ref, ref, hx_s.at[0], hx_r.at[g, i, j - 1], {"tp": hop(j) * 2 + core})

    def hid_pair(g, i):
        at = pl.multiple_of((i * tp + core * chips) * n_tile, 128)
        ref = hid.at[group(g), pl.ds(at, chips * n_tile)]
        return remote(ref, ref, hp_s.at[0], hp_r.at[g, i], {"tp": partner})

    def send_tile(g, i):
        for j in range(1, chips):
            hid_x(g, i, j).start()

    def send_hidden(g, first):
        for i in range(first, tiles):
            send_tile(g, i)

    def gate_up(g, sent=tiles):
        feat_pair(g).wait_recv()
        batch = max(u for u in range(1, 6) if (group_rows // 16) % u == 0)

        def norm(i, carry):
            for u in range(batch):
                here = (i * batch + u) * 16
                span = pl.ds(pl.multiple_of(g * group_rows + here, 16), 16)
                x = feats[span, :].astype(f32)
                square = jnp.sum(x * x, axis=1, keepdims=True)
                x = x * lax.rsqrt(square / (width * tp) + epsilon) * gain[...]
                rows_in[pl.ds(pl.multiple_of(here, 16), 16), :] = x.astype(bf16)
            return carry

        lax.fori_loop(0, group_rows // (16 * batch), norm, 0)

        def tile(i, send):
            cols = pl.ds(pl.multiple_of(i * n_tile, 128), n_tile)
            x = rows_in[...]
            gate = jnp.dot(x, wg[:, cols], preferred_element_type=f32)
            upper = jnp.dot(x, wu[:, cols], preferred_element_type=f32)
            value = gate / (1.0 + jnp.exp(-gate)) * upper
            hid[group(g), pl.ds(tile_at(i, ti), n_tile)] = value.astype(bf16)
            if send:
                send_tile(g, i)

        def loop(first, last, send):
            def body(i, carry):
                tile(i, send)
                return carry

            if last > first:
                lax.fori_loop(first, last, body, 0)

        loop(0, sent, True)
        loop(sent, tiles, False)

    def return_copy(d):
        return remote(back.at[block(d)], ret.at[block(d)], r_s.at[0], r_r.at[d - 1], {"ep": flip(me, d)})

    def relay(g, first=0, last=tiles):
        for i in range(first, last):
            for j in range(1, chips):
                hid_x(g, i, j).wait_recv()
            hid_pair(g, i).start()

    out_tile = min(256, width)

    def down(g, first=0, last=tiles, start=None, stop=True):
        for i in range(first, last):
            hid_pair(g, i).wait_recv()
        deep = pl.ds(first * tp * n_tile, (last - first) * tp * n_tile)

        def body(i, carry):
            cols = pl.ds(pl.multiple_of(i * out_tile, 128), out_tile)
            value = jnp.dot(hid[group(g), deep], wd[deep, cols], preferred_element_type=f32)
            if start is not None:
                value = value + start[:, cols]
            if stop:
                back[group(g), cols] = value.astype(bf16)
            else:
                part[:, cols] = value
            return carry

        lax.fori_loop(0, width // out_tile, body, 0)
        if stop:
            for d in members(g):
                if d > 0:
                    return_copy(d).start()
                else:
                    ret[block(0), :] = back[block(0), :]

    def piece_slots(piece):
        return pl.ds(piece[0] * group_rows, piece[1] * group_rows)

    def combine(q):
        piece, pick = pieces[q], picks[q]
        for g in range(piece[0], sum(piece)):
            for d in members(g):
                if d > 0:
                    return_copy(d).wait_recv()
        value = 0.0 if q == 0 else mix[...]
        for k in range(2):
            found = jnp.dot(pick[k], ret[piece_slots(piece), :], preferred_element_type=f32)
            value = value + found * wide(wcol[k], width)
        mix[...] = value

    for j in range(1, tp):
        meet_tp(j)
    for j in range(1, chips):
        token_copy(j).start()
    gain[:, own] = pre_ref[...]
    for j in range(1, tp):
        gain_copy(j).start()
    for g in (4, 5, 1, 2, 3, 6, 7):
        pick_own(g)
        send_own(g)
    pick_own(0)
    send_own(0)
    for k in range(2):
        column = to_column(target[k])
        wcol[k] = to_column(rw_ref[k : k + 1, :])
        for piece, pick in zip(pieces, picks):
            base = piece[0] * group_rows
            for at in range(0, pick.shape[2], 128):
                size = min(128, pick.shape[2] - at)
                lane = lax.broadcasted_iota(jnp.int32, (rows, size), 1).astype(f32)
                pick[k, :, at : at + size] = jnp.where(
                    column[:, 0:size] == lane + float(base + at), 1.0, 0.0
                ).astype(bf16)
    for j in range(1, chips):
        token_copy(j).wait_recv()
    send_rest(0)
    take(0)
    for g in (1, 6, 7, 2, 3):
        send_rest(g)
    take(4)
    for load in loads[:2]:
        load.wait()
    for j in range(1, tp):
        gain_copy(j).wait_recv()
    gate_up(0, early)
    take(5)
    take(1)
    pass_on(4)
    gate_up(1)
    pass_on(5)
    relay(0, 0, early)
    gate_up(4)
    loads[2].wait()
    if early:
        down(0, 0, early, stop=False)
    take(6)
    gate_up(5)
    relay(1)
    take(7)
    gate_up(6)
    down(1)
    relay(4)
    take(2)
    gate_up(7)
    down(4)
    relay(5)
    take(3)
    gate_up(2)
    down(5)
    relay(6)
    gate_up(3)
    send_hidden(0, early)
    down(6)
    relay(7)
    down(7)
    relay(2)
    down(2)
    combine(0)
    relay(3)
    down(3)
    relay(0, early)
    combine(1)
    down(0, early, start=part if early else None)
    combine(2)
    mixed = mix[...]
    ss_out[0] = row_sums(mixed * mixed)
    out_copies = [
        remote(ss_out.at[0], ss_out.at[j], so_s.at[0], so_r.at[j - 1], {"tp": (ti + j) % tp})
        for j in range(1, tp)
    ]
    for copy in out_copies:
        copy.start()

    def drain(ref, sem):
        remote(ref, ref, sem.at[0], so_r.at[0], {"tp": partner}).wait_send()

    later = pl.ds(cap, (n - 1) * cap)
    fresh = (groups - len(shared)) * per_group - 1
    drain(tok_x.at[:, 0 : (chips - 1) * width], t_s)
    drain(outg.at[later, 0:width], d_s)
    drain(outg.at[0 : fresh * cap, 0 : (chips - 1) * width], d_s)
    drain(back.at[later], r_s)
    drain(gain.at[:, 0 : (tp - 1) * width], g_s)
    if shared:
        drain(feats.at[0 : len(shared) * group_rows, 0 : (chips - 1) * width], fx_s)
    drain(feats.at[:, 0:side], fp_s)
    drain(hid.at[:, 0 : (chips - 1) * units], hx_s)
    drain(hid.at[:, 0 : chips * units], hp_s)
    for copy in out_copies:
        copy.wait_recv()
    total = ss_out[0]
    for j in range(1, tp):
        total = total + ss_out[j]
    scale = wide(to_column(lax.rsqrt(total / (width * tp) + epsilon)), width)
    out_ref[...] = (mixed * scale * post_ref[...]).astype(bf16)
    drain(ss_out.at[0 : tp - 1], so_s)


def on_device(
    tokens, expert_ids, route_weights, pre_gain, post_gain, gate_weight, up_weight, down_weight
):
    rows, width = tokens.shape
    n, tp = lax.axis_size("ep"), lax.axis_size("tp")
    assert gate_weight.shape[0] == 1 and expert_ids.shape[1] == 2
    capacity = max(2, rows * 2 * 5 // (4 * n))
    cap = -(-capacity // 16) * 16
    groups = 8
    assert n % groups == 0
    shared = (4, 5)
    pieces = ((4, 4), (1, 3), (0, 1))
    slots = n * cap
    chips = tp // 2
    features, units = gate_weight.shape[1:]
    hidden_all = units * tp
    tiles = units // min(256, units)
    early = tiles // 2
    group_rows = slots // groups
    dma, regular = pltpu.SemaphoreType.DMA, pltpu.SemaphoreType.REGULAR
    vmem = pl.BlockSpec(memory_space=pltpu.VMEM)
    hbm = pl.BlockSpec(memory_space=pl.ANY)
    return pl.pallas_call(
        functools.partial(kernel, n, tp, cap, groups, shared, early, pieces),
        out_shape=jax.ShapeDtypeStruct((rows, width), bf16),
        in_specs=[vmem] * 5 + [hbm] * 3,
        out_specs=vmem,
        scratch_shapes=[
            pltpu.VMEM((features, units), bf16),
            pltpu.VMEM((features, units), bf16),
            pltpu.VMEM((hidden_all, width), bf16),
            pltpu.VMEM((rows, chips * width), bf16),
            pltpu.VMEM((slots, chips * width), bf16),
            pltpu.VMEM((slots, features), bf16),
            pltpu.VMEM((group_rows, features), bf16),
            pltpu.VMEM((slots, hidden_all), bf16),
            pltpu.VMEM((group_rows, width), f32),
            pltpu.VMEM((slots, width), bf16),
            pltpu.VMEM((slots, width), bf16),
            pltpu.VMEM((1, features), f32),
            pltpu.VMEM((tp, 1, rows), f32),
            pltpu.VMEM((rows, width), f32),
            pltpu.VMEM((2, rows, 128), f32),
            *[pltpu.VMEM((2, rows, count * group_rows), bf16) for _, count in pieces],
            dma((3,)),
            regular((n - 1,)), regular((tp - 1,)),
            dma((1,)), dma((chips - 1,)),
            dma((1,)), dma((tp - 1,)), dma((1,)), dma((tp - 1,)),
            dma((1,)), dma((n - 1, chips)),
            dma((1,)), dma((groups, chips - 1)),
            dma((1,)), dma((groups,)),
            dma((1,)), dma((groups, tiles, chips - 1)),
            dma((1,)), dma((groups, tiles)),
            dma((1,)), dma((n - 1,)),
        ],
        compiler_params=pltpu.CompilerParams(
            collective_id=0, has_side_effects=True, vmem_limit_bytes=56 * 1024 * 1024
        ),
    )(
        tokens, jnp.transpose(expert_ids), jnp.transpose(route_weights),
        pre_gain.reshape(1, -1), post_gain.reshape(1, -1),
        gate_weight, up_weight, down_weight,
    )


def solution(mesh):
    return jax.shard_map(
        on_device,
        mesh=mesh,
        in_specs=(
            P("ep", "tp"),
            P("ep", None),
            P("ep", None),
            P("tp"),
            P("tp"),
            P("ep", None, "tp"),
            P("ep", None, "tp"),
            P("ep", None, "tp"),
        ),
        out_specs=P("ep", "tp"),
        check_vma=False,
    )
```

time: 64.5 us -> 66.6 us (1.033)
  Pallas kernels: 62.7 us -> 64.8 us
    pallas_call x1, Pallas kernels: 62.7 us -> 64.8 us  [on_device(): pl.pallas_call(functools.partial(kernel, n, tp, cap, groups, shared, earl...]
where the time goes in v1:
time: 66.6 us; the launch traced here: 66.5 us
  Pallas kernels  64.8 us (97%)
  local copies, waits for them, and re-layouts  1.67 us (3%)
    pallas_call x1, Pallas kernels, on_device(): pl.pallas_call(functools.partial(kernel, n, tp, cap, groups, shared, earl...  64.8 us
    unnamed x1, local copies, waits for them, and re-layouts  1.67 us

profile of v1, /device:TPU:0, one launch (start us, length us, event | category | flops | bytes accessed | tf_op | source)
XLA Modules:
  0.0 66.5 jit_solution(3667753804968927394)
XLA Ops:
  0.0 64.8 %shard_map.82 = bf16[256,512]{1,0:T(8,128)(2,1)} custom-call(bf16[256,512]{1,0:T(8,128)(2,1)} %tok_ref.1, s32[2,256]{1,0:T(2,128)} %bitcast.4, f32[2,256]{1,0:T(2,128)} %bitcast.5, f32[1,512]{1,0:T(1,128)} %bitcast.6, f32[1,512]{1,0:T(1,128)} %bitcast.7, bf16[1,2048,1024]{2,1,0:T(8,128)(2,1)} %wg_hbm.1, bf16[1,2048,1024]{2,1,0:T(8,128)(2,1)} %wu_hbm.1, ...), custom_call_target="tpu_custom_call" | custom-call | tf_op jit(solution)/shard_map/pallas_call | solution.py:451
  64.8 1.7 %copy.10 = bf16[256,512]{1,0:T(8,128)(2,1)} copy(bf16[256,512]{1,0:T(8,128)(2,1)} %shard_map.82) | data formatting | bytes 524288

commit v2 on v1

v2 whole, which is shorter than its diff:
```python
import functools

import jax
import jax.numpy as jnp
from jax import lax
from jax.experimental import pallas as pl
from jax.experimental.pallas import tpu as pltpu
from jax.sharding import PartitionSpec as P

epsilon = 1e-06
MESH = pl.DeviceIdType.MESH
f32, bf16 = jnp.float32, jnp.bfloat16


def flip(index, bits):
    out, bit = index, 1
    while bit <= bits:
        if bits & bit:
            out = out + bit * (1 - 2 * ((index // bit) % 2))
        bit *= 2
    return out


def to_column(row):
    return jnp.transpose(jnp.broadcast_to(row, (128, row.shape[1])))


def wide(column, width):
    return jnp.concatenate([column] * (width // 128), axis=1)


def row_sums(values):
    part = values[:, 0:128]
    for at in range(128, values.shape[1], 128):
        part = part + values[:, at : at + 128]
    return jnp.sum(jnp.transpose(part), axis=0, keepdims=True)


def kernel(
    n, tp, cap, groups, crossed, early, pieces,
    tok_hbm, ids_hbm, rw_hbm, pre_hbm, post_hbm, wg_hbm, wu_hbm, wd_hbm,
    out_ref,
    tok_ref, ids_ref, rw_ref, pre_ref, post_ref, wg, wu, wd, outg, over, feats, rows_in, hid, part, back, ret, gain, ss_out, mix, wcol, *rest,
):
    hots, sems = rest[: len(pieces)], rest[len(pieces) :]
    (i_sem, w_sem, met_ep, met_tp, g_s, g_r, so_s, so_r, c_s, c_r, d_s, d_r, d_x, fx_s, fx_r, fp_s, fp_r,
     hx_s, hx_r, hp_s, hp_r, r_s, r_r) = sems
    me, ti = lax.axis_index("ep"), lax.axis_index("tp")
    chips = tp // 2
    chip, core = ti // 2, ti % 2
    partner = chip * 2 + (1 - core)
    rows, width = tok_ref.shape
    side = chips * width
    units = wg.shape[1]
    n_tile = min(256, units)
    tiles = units // n_tile
    per_group = n // groups
    group_rows = per_group * cap

    barrier = pltpu.get_barrier_semaphore()

    def signal(sem, where):
        pl.semaphore_signal(sem, inc=1, device_id=where, device_id_type=MESH)

    for j in range(1, tp):
        peer = (ti + j) % tp
        pl.when(peer > ti)(functools.partial(signal, barrier, {"tp": peer}))
    for d in range(1, n):
        peer = flip(me, d)
        pl.when(peer > me)(functools.partial(signal, barrier, {"ep": peer}))

    inputs = [
        pltpu.make_async_copy(src, dst, i_sem.at[i])
        for i, (src, dst) in enumerate((
            (ids_hbm, ids_ref), (tok_hbm, tok_ref), (pre_hbm, pre_ref), (rw_hbm, rw_ref),
            (post_hbm, post_ref),
        ))
    ]
    for copy in inputs:
        copy.start()

    def load_all(src, dst, sem, step, place):
        for at in range(0, dst.shape[0], step):
            pltpu.make_async_copy(
                src.at[0, pl.ds(at, step)], dst.at[pl.ds(place(at // step) * step, step)], sem
            ).start()

    def position(owner):
        return owner % 2 * chips + owner // 2

    pl.when(me + ti > 0)(lambda: pl.semaphore_wait(barrier, me + ti))
    for j in range(1, tp):
        peer = (ti + j) % tp
        pl.when(peer < ti)(functools.partial(signal, met_tp.at[tp - j - 1], {"tp": peer}))
    for d in range(1, n):
        peer = flip(me, d)
        pl.when(peer < me)(functools.partial(signal, met_ep.at[d - 1], {"ep": peer}))

    load_all(wg_hbm, wg, w_sem.at[0], width, position)
    load_all(wu_hbm, wu, w_sem.at[1], width, position)
    load_all(
        wd_hbm, wd, w_sem.at[2], n_tile, lambda at: at % tiles * tp + position(at // tiles)
    )
    loads = [
        pltpu.make_async_copy(src.at[0], dst, w_sem.at[i])
        for i, (src, dst) in enumerate(((wg_hbm, wg), (wu_hbm, wu), (wd_hbm, wd)))
    ]

    def meet_tp(j):
        pl.when((ti + j) % tp > ti)(lambda: pl.semaphore_wait(met_tp.at[j - 1], 1))

    def meet_ep(d):
        pl.when(flip(me, d) > me)(lambda: pl.semaphore_wait(met_ep.at[d - 1], 1))

    def remote(src, dst, s_sem, r_sem, where):
        return pltpu.make_async_remote_copy(
            src_ref=src, dst_ref=dst, send_sem=s_sem, recv_sem=r_sem,
            device_id=where, device_id_type=MESH,
        )

    inputs[0].wait()
    lanes = max(n, 16)
    rel = [jnp.bitwise_xor(ids_ref[k : k + 1, :], me) for k in range(2)]
    d_iota = lax.broadcasted_iota(jnp.int32, (lanes, rows), 0)
    hot = [jnp.where(rel[k] == d_iota, 1.0, 0.0).astype(f32) for k in range(2)]
    earlier = jnp.where(
        lax.broadcasted_iota(jnp.int32, (rows, rows), 0)
        < lax.broadcasted_iota(jnp.int32, (rows, rows), 1), 1.0, 0.0,
    ).astype(bf16)
    prefix = jnp.dot((hot[0] + hot[1]).astype(bf16), earlier, preferred_element_type=f32)
    target = [
        rel[k].astype(f32) * cap + jnp.sum(prefix * hot[k], axis=0, keepdims=True)
        for k in range(2)
    ]
    slot_iota = lax.broadcasted_iota(jnp.int32, (cap, rows), 0).astype(f32)

    def hop(j):
        return (chip + j) % chips

    def seg(j):
        return pl.ds(pl.multiple_of(core * side + hop(j) * width, 128), width)

    own = seg(0)
    half = pl.ds(pl.multiple_of(core * side, 128), side)

    def block(d):
        return pl.ds(d * cap, cap)

    def group(g):
        return pl.ds(g * group_rows, group_rows)

    def members(g):
        return range(g * per_group, (g + 1) * per_group)

    def gain_copy(j):
        return remote(pre_ref, gain.at[:, own], g_s.at[0], g_r.at[j - 1], {"tp": (ti + j) % tp})

    def dispatch_copy(d):
        return remote(
            outg.at[block(d)], feats.at[block(d), own], d_s.at[0], d_r.at[d - 1], {"ep": flip(me, d)}
        )

    def cross_copy(g, j):
        return remote(
            outg.at[group(g)], over.at[crossed.index(g), chip],
            c_s.at[0], c_r.at[g, j - 1], {"tp": hop(j) * 2 + core},
        )

    def forward_copy(d, j):
        g, source = d // per_group, hop(chips - j)
        return remote(
            over.at[crossed.index(g), source, pl.ds(d % per_group * cap, cap)],
            feats.at[block(d), seg(chips - j)],
            d_s.at[0], d_x.at[d - 1, j - 1], {"ep": flip(me, d)},
        )

    def feat_x(g, j):
        ref = feats.at[group(g), own]
        return remote(ref, ref, fx_s.at[0], fx_r.at[g, j - 1], {"tp": hop(j) * 2 + core})

    def feat_pair(g):
        ref = feats.at[group(g), half]
        return remote(ref, ref, fp_s.at[0], fp_r.at[g], {"tp": partner})

    def choose(d):
        base = float(d * cap)
        chosen = jnp.where(
            (target[0] == slot_iota + base) | (target[1] == slot_iota + base), 1.0, 0.0
        ).astype(bf16)
        picked = jnp.dot(chosen, tok_ref[...], preferred_element_type=f32).astype(bf16)
        if d == 0:
            feats[block(0), own] = picked
        else:
            outg[block(d), :] = picked

    def pick(g):
        for d in members(g):
            choose(d)

    def send(g):
        for d in members(g):
            if d > 0:
                meet_ep(d)
                dispatch_copy(d).start()

    def cross(g):
        for j in range(1, chips):
            cross_copy(g, j).start()

    def forward(g):
        for j in range(1, chips):
            cross_copy(g, j).wait_recv()
            for d in members(g):
                forward_copy(d, j).start()

    def share(g):
        for d in members(g):
            if d > 0:
                dispatch_copy(d).wait_recv()
        for j in range(1, chips):
            feat_x(g, j).start()

    def pass_on(g):
        for j in range(1, chips):
            if g not in crossed:
                feat_x(g, j).wait_recv()
                continue
            for d in members(g):
                if j == 1:
                    dispatch_copy(d).wait_recv()
                forward_copy(d, j).wait_recv()
        feat_pair(g).start()

    def tile_at(i, owner):
        return pl.multiple_of((i * tp + position(owner)) * n_tile, 128)

    def hid_x(g, i, j):
        ref = hid.at[group(g), pl.ds(tile_at(i, ti), n_tile)]
        return remote(ref, ref, hx_s.at[0], hx_r.at[g, i, j - 1], {"tp": hop(j) * 2 + core})

    def hid_pair(g, i):
        at = pl.multiple_of((i * tp + core * chips) * n_tile, 128)
        ref = hid.at[group(g), pl.ds(at, chips * n_tile)]
        return remote(ref, ref, hp_s.at[0], hp_r.at[g, i], {"tp": partner})

    def send_tile(g, i):
        for j in range(1, chips):
            hid_x(g, i, j).start()

    def send_hidden(g, first):
        for i in range(first, tiles):
            send_tile(g, i)

    def gate_up(g, many=1, sent=tiles):
        for at in range(g, g + many):
            feat_pair(at).wait_recv()
        count = many * group_rows
        span = pl.ds(g * group_rows, count)
        batch = max(u for u in range(1, 6) if (count // 16) % u == 0)

        def norm(i, carry):
            for u in range(batch):
                here = (i * batch + u) * 16
                here_rows = pl.ds(pl.multiple_of(g * group_rows + here, 16), 16)
                x = feats[here_rows, :].astype(f32)
                square = jnp.sum(x * x, axis=1, keepdims=True)
                x = x * lax.rsqrt(square / (width * tp) + epsilon) * gain[...]
                rows_in[pl.ds(pl.multiple_of(here, 16), 16), :] = x.astype(bf16)
            return carry

        lax.fori_loop(0, count // (16 * batch), norm, 0)

        def tile(i, send):
            cols = pl.ds(pl.multiple_of(i * n_tile, 128), n_tile)
            x = rows_in[0:count, :]
            gate = jnp.dot(x, wg[:, cols], preferred_element_type=f32)
            upper = jnp.dot(x, wu[:, cols], preferred_element_type=f32)
            value = gate / (1.0 + jnp.exp(-gate)) * upper
            hid[span, pl.ds(tile_at(i, ti), n_tile)] = value.astype(bf16)
            if send:
                for at in range(g, g + many):
                    send_tile(at, i)

        def loop(first, last, send):
            def body(i, carry):
                tile(i, send)
                return carry

            if last > first:
                lax.fori_loop(first, last, body, 0)

        loop(0, sent, True)
        loop(sent, tiles, False)

    def return_copy(d):
        return remote(back.at[block(d)], ret.at[block(d)], r_s.at[0], r_r.at[d - 1], {"ep": flip(me, d)})

    def relay(g, many=1, first=0, last=tiles):
        for i in range(first, last):
            for at in range(g, g + many):
                for j in range(1, chips):
                    hid_x(at, i, j).wait_recv()
                hid_pair(at, i).start()

    out_tile = min(256, width)

    def down(g, many=1, first=0, last=tiles, start=None, stop=True):
        for i in range(first, last):
            for at in range(g, g + many):
                hid_pair(at, i).wait_recv()
        span = pl.ds(g * group_rows, many * group_rows)
        deep = pl.ds(first * tp * n_tile, (last - first) * tp * n_tile)

        def body(i, carry):
            cols = pl.ds(pl.multiple_of(i * out_tile, 128), out_tile)
            value = jnp.dot(hid[span, deep], wd[deep, cols], preferred_element_type=f32)
            if start is not None:
                value = value + start[:, cols]
            if stop:
                back[span, cols] = value.astype(bf16)
            else:
                part[:, cols] = value
            return carry

        lax.fori_loop(0, width // out_tile, body, 0)
        if stop:
            for d in range(g * per_group, (g + many) * per_group):
                if d > 0:
                    return_copy(d).start()
                else:
                    ret[block(0), :] = back[block(0), :]

    def piece_slots(piece):
        return pl.ds(piece[0] * group_rows, piece[1] * group_rows)

    def combine(q):
        piece, hot_rows = pieces[q], hots[q]
        for g in range(piece[0], sum(piece)):
            for d in members(g):
                if d > 0:
                    return_copy(d).wait_recv()
        value = 0.0 if q == 0 else mix[...]
        for k in range(2):
            found = jnp.dot(hot_rows[k], ret[piece_slots(piece), :], preferred_element_type=f32)
            value = value + found * wide(wcol[k], width)
        mix[...] = value

    inputs[1].wait()
    pick(5)
    pick(7)
    pick(4)
    pick(0)
    pick(2)
    pick(1)
    for j in range(1, tp):
        meet_tp(j)
    send(1)
    cross(1)
    send(4)
    share(0)
    cross(2)
    pick(3)
    send(2)
    pick(6)
    cross(3)
    forward(1)
    share(4)
    send(6)
    pass_on(0)
    inputs[2].wait()
    gain[:, own] = pre_ref[...]
    for j in range(1, tp):
        gain_copy(j).start()
    pass_on(1)
    send(5)
    forward(2)
    for load in loads[:2]:
        load.wait()
    for j in range(1, tp):
        gain_copy(j).wait_recv()
    gate_up(1)
    for copy in inputs[3:]:
        copy.wait()
    for k in range(2):
        column = to_column(target[k])
        wcol[k] = to_column(rw_ref[k : k + 1, :])
        for piece, hot_rows in zip(pieces, hots):
            base = piece[0] * group_rows
            for at in range(0, hot_rows.shape[2], 128):
                size = min(128, hot_rows.shape[2] - at)
                lane = lax.broadcasted_iota(jnp.int32, (rows, size), 1).astype(f32)
                hot_rows[k, :, at : at + size] = jnp.where(
                    column[:, 0:size] == lane + float(base + at), 1.0, 0.0
                ).astype(bf16)
    gate_up(0, 1, early)
    send(7)
    share(5)
    send(3)
    relay(1)
    pass_on(4)
    relay(0, 1, 0, early)
    share(6)
    gate_up(4)
    loads[2].wait()
    down(1)
    share(7)
    pass_on(5)
    pass_on(6)
    forward(3)
    gate_up(5)
    relay(4)
    combine(0)
    gate_up(6)
    pass_on(7)
    pass_on(2)
    down(4)
    if early:
        down(0, 1, 0, early, stop=False)
    relay(5)
    pass_on(3)
    gate_up(7)
    down(5)
    relay(6)
    gate_up(2)
    down(6)
    relay(7)
    gate_up(3)
    down(7)
    relay(2)
    down(2)
    relay(3)
    send_hidden(0, early)
    down(3)
    relay(0, 1, early)
    combine(1)
    down(0, 1, early, start=part if early else None)
    combine(4)
    combine(2)
    combine(3)
    mixed = mix[...]
    ss_out[0] = row_sums(mixed * mixed)
    out_copies = [
        remote(ss_out.at[0], ss_out.at[j], so_s.at[0], so_r.at[j - 1], {"tp": (ti + j) % tp})
        for j in range(1, tp)
    ]
    for copy in out_copies:
        copy.start()
    mix[...] = mixed * post_ref[...]

    def drain(ref, sem):
        remote(ref, ref, sem.at[0], so_r.at[0], {"tp": partner}).wait_send()

    slots = n * cap
    later = pl.ds(cap, slots - cap)
    drain(outg.at[later], d_s)
    drain(back.at[later], r_s)
    drain(gain.at[:, 0 : (tp - 1) * width], g_s)
    crossing = len(crossed) * group_rows
    shared = pl.ds(0, slots - crossing)
    drain(feats.at[shared, 0 : (chips - 1) * width], fx_s)
    if crossed:
        drain(feats.at[0:crossing, 0 : (chips - 1) * width], c_s)
        drain(feats.at[0:crossing, 0 : (chips - 1) * width], d_s)
    drain(feats.at[:, 0:side], fp_s)
    drain(hid.at[:, 0 : (chips - 1) * units], hx_s)
    drain(hid.at[:, 0 : chips * units], hp_s)
    for copy in out_copies:
        copy.wait_recv()
    total = ss_out[0]
    for j in range(1, tp):
        total = total + ss_out[j]
    scale = wide(to_column(lax.rsqrt(total / (width * tp) + epsilon)), width)
    out_ref[...] = (mix[...] * scale).astype(bf16)
    drain(ss_out.at[0 : tp - 1], so_s)


def on_device(
    tokens, expert_ids, route_weights, pre_gain, post_gain, gate_weight, up_weight, down_weight
):
    rows, width = tokens.shape
    n, tp = lax.axis_size("ep"), lax.axis_size("tp")
    assert gate_weight.shape[0] == 1 and expert_ids.shape[1] == 2
    capacity = max(2, rows * 2 * 5 // (4 * n))
    cap = -(-capacity // 16) * 16
    groups = 8
    assert n % groups == 0
    crossed = (1, 2, 3)
    pieces = ((1, 1), (4, 2), (0, 1), (2, 2), (6, 2))
    slots = n * cap
    chips = tp // 2
    features, units = gate_weight.shape[1:]
    hidden_all = units * tp
    tiles = units // min(256, units)
    early = tiles // 2
    group_rows = slots // groups
    dma, regular = pltpu.SemaphoreType.DMA, pltpu.SemaphoreType.REGULAR
    vmem = pl.BlockSpec(memory_space=pltpu.VMEM)
    hbm = pl.BlockSpec(memory_space=pl.ANY)
    return pl.pallas_call(
        functools.partial(kernel, n, tp, cap, groups, crossed, early, pieces),
        out_shape=pltpu.VMEM((rows, width), bf16),
        in_specs=[hbm] * 8,
        out_specs=vmem,
        scratch_shapes=[
            pltpu.VMEM((rows, width), bf16),
            pltpu.VMEM((2, rows), jnp.int32),
            pltpu.VMEM((2, rows), f32),
            pltpu.VMEM((1, width), f32),
            pltpu.VMEM((1, width), f32),
            pltpu.VMEM((features, units), bf16),
            pltpu.VMEM((features, units), bf16),
            pltpu.VMEM((hidden_all, width), bf16),
            pltpu.VMEM((slots, width), bf16),
            pltpu.VMEM((max(1, len(crossed)), chips, group_rows, width), bf16),
            pltpu.VMEM((slots, features), bf16),
            pltpu.VMEM((2 * group_rows, features), bf16),
            pltpu.VMEM((slots, hidden_all), bf16),
            pltpu.VMEM((group_rows, width), f32),
            pltpu.VMEM((slots, width), bf16),
            pltpu.VMEM((slots, width), bf16),
            pltpu.VMEM((1, features), f32),
            pltpu.VMEM((tp, 1, rows), f32),
            pltpu.VMEM((rows, width), f32),
            pltpu.VMEM((2, rows, 128), f32),
            *[pltpu.VMEM((2, rows, count * group_rows), bf16) for _, count in pieces],
            dma((5,)), dma((3,)),
            regular((n - 1,)), regular((tp - 1,)),
            dma((1,)), dma((tp - 1,)), dma((1,)), dma((tp - 1,)),
            dma((1,)), dma((groups, chips - 1)),
            dma((1,)), dma((n - 1,)), dma((n - 1, chips - 1)),
            dma((1,)), dma((groups, chips - 1)),
            dma((1,)), dma((groups,)),
            dma((1,)), dma((groups, tiles, chips - 1)),
            dma((1,)), dma((groups, tiles)),
            dma((1,)), dma((n - 1,)),
        ],
        compiler_params=pltpu.CompilerParams(
            collective_id=0, has_side_effects=True, vmem_limit_bytes=56 * 1024 * 1024
        ),
    )(
        tokens, jnp.transpose(expert_ids), jnp.transpose(route_weights),
        pre_gain.reshape(1, -1), post_gain.reshape(1, -1),
        gate_weight, up_weight, down_weight,
    )


def solution(mesh):
    return jax.shard_map(
        on_device,
        mesh=mesh,
        in_specs=(
            P("ep", "tp"),
            P("ep", None),
            P("ep", None),
            P("tp"),
            P("tp"),
            P("ep", None, "tp"),
            P("ep", None, "tp"),
            P("ep", None, "tp"),
        ),
        out_specs=P("ep", "tp"),
        check_vma=False,
    )
```

time: 66.6 us -> 61.1 us (0.917)
  Pallas kernels: 64.8 us -> 60.3 us
  local copies, waits for them, and re-layouts: 1.67 us -> 0.71 us
    pallas_call x1, Pallas kernels: 64.8 us -> 60.3 us  [on_device(): pl.pallas_call(functools.partial(kernel, n, tp, cap, groups, crossed, ear...]
    unnamed x1, local copies, waits for them, and re-layouts: 1.67 us -> 0.71 us
where the time goes in v2:
time: 61.1 us; the launch traced here: 61 us
  Pallas kernels  60.3 us (99%)
  local copies, waits for them, and re-layouts  0.71 us (1%)
    pallas_call x1, Pallas kernels, on_device(): pl.pallas_call(functools.partial(kernel, n, tp, cap, groups, crossed, ear...  60.3 us

profile of v2, /device:TPU:0, one launch (start us, length us, event | category | flops | bytes accessed | tf_op | source)
XLA Modules:
  0.0 61.0 jit_solution(4486906642287555962)
XLA Ops:
  0.0 60.3 %shard_map.82 = bf16[256,512]{1,0:T(8,128)(2,1)S(1)} custom-call(bf16[256,512]{1,0:T(8,128)(2,1)} %tok_hbm.1, s32[2,256]{1,0:T(2,128)} %bitcast.4, f32[2,256]{1,0:T(2,128)} %bitcast.5, f32[1,512]{1,0:T(1,128)} %bitcast.6, f32[1,512]{1,0:T(1,128)} %bitcast.7, bf16[1,2048,1024]{2,1,0:T(8,128)(2,1)} %wg_hbm.1, bf16[1,2048,1024]{2,1,0:T(8,128)(2,1)} %wu_hbm.1, ...), custom_call_target="tpu_custom_call" | custom-call | tf_op jit(solution)/shard_map/pallas_call | solution.py:499
  60.3 0.7 %copy.10 = bf16[256,512]{1,0:T(8,128)(2,1)} copy(bf16[256,512]{1,0:T(8,128)(2,1)S(1)} %shard_map.82) | data formatting | bytes 524288

commit v3 on v2

--- a/solution.py
+++ b/solution.py
@@ -346,39 +346,40 @@
         mix[...] = value
 
     inputs[1].wait()
-    pick(5)
+    pick(4)
     pick(7)
-    pick(4)
     pick(0)
+    pick(1)
+    pick(6)
     pick(2)
-    pick(1)
     for j in range(1, tp):
         meet_tp(j)
+    cross(1)
+    share(0)
+    send(4)
+    pick(5)
     send(1)
-    cross(1)
-    send(4)
-    share(0)
     cross(2)
     pick(3)
+    forward(1)
+    cross(3)
     send(2)
-    pick(6)
-    cross(3)
-    forward(1)
-    share(4)
-    send(6)
-    pass_on(0)
     inputs[2].wait()
     gain[:, own] = pre_ref[...]
     for j in range(1, tp):
         gain_copy(j).start()
+    send(6)
+    share(4)
+    send(5)
+    pass_on(0)
     pass_on(1)
-    send(5)
-    forward(2)
     for load in loads[:2]:
         load.wait()
     for j in range(1, tp):
         gain_copy(j).wait_recv()
     gate_up(1)
+    send(3)
+    send(7)
     for copy in inputs[3:]:
         copy.wait()
     for k in range(2):
@@ -393,29 +394,28 @@
                     column[:, 0:size] == lane + float(base + at), 1.0, 0.0
                 ).astype(bf16)
     gate_up(0, 1, early)
-    send(7)
     share(5)
-    send(3)
+    pass_on(4)
     relay(1)
-    pass_on(4)
+    forward(2)
     relay(0, 1, 0, early)
     share(6)
     gate_up(4)
     loads[2].wait()
     down(1)
-    share(7)
-    pass_on(5)
-    pass_on(6)
-    forward(3)
-    gate_up(5)
-    relay(4)
-    combine(0)
-    gate_up(6)
-    pass_on(7)
-    pass_on(2)
-    down(4)
     if early:
         down(0, 1, 0, early, stop=False)
+    pass_on(5)
+    share(7)
+    pass_on(6)
+    gate_up(5)
+    forward(3)
+    gate_up(6)
+    combine(0)
+    pass_on(2)
+    relay(4)
+    pass_on(7)
+    down(4)
     relay(5)
     pass_on(3)
     gate_up(7)
@@ -427,9 +427,9 @@
     gate_up(3)
     down(7)
     relay(2)
+    send_hidden(0, early)
     down(2)
     relay(3)
-    send_hidden(0, early)
     down(3)
     relay(0, 1, early)
     combine(1)

time: 61.1 us -> 59.4 us (0.972)
  Pallas kernels: 60.3 us -> 58.6 us
    pallas_call x1, Pallas kernels: 60.3 us -> 58.6 us  [on_device(): pl.pallas_call(functools.partial(kernel, n, tp, cap, groups, crossed, ear...]
where the time goes in v3:
time: 59.4 us; the launch traced here: 59.3 us
  Pallas kernels  58.6 us (99%)
  local copies, waits for them, and re-layouts  0.71 us (1%)
    pallas_call x1, Pallas kernels, on_device(): pl.pallas_call(functools.partial(kernel, n, tp, cap, groups, crossed, ear...  58.6 us

profile of v3, /device:TPU:0, one launch (start us, length us, event | category | flops | bytes accessed | tf_op | source)
XLA Modules:
  0.0 59.3 jit_solution(12361324157331797693)
XLA Ops:
  0.0 58.6 %shard_map.82 = bf16[256,512]{1,0:T(8,128)(2,1)S(1)} custom-call(bf16[256,512]{1,0:T(8,128)(2,1)} %tok_hbm.1, s32[2,256]{1,0:T(2,128)} %bitcast.4, f32[2,256]{1,0:T(2,128)} %bitcast.5, f32[1,512]{1,0:T(1,128)} %bitcast.6, f32[1,512]{1,0:T(1,128)} %bitcast.7, bf16[1,2048,1024]{2,1,0:T(8,128)(2,1)} %wg_hbm.1, bf16[1,2048,1024]{2,1,0:T(8,128)(2,1)} %wu_hbm.1, ...), custom_call_target="tpu_custom_call" | custom-call | tf_op jit(solution)/shard_map/pallas_call | solution.py:499
  58.6 0.7 %copy.10 = bf16[256,512]{1,0:T(8,128)(2,1)} copy(bf16[256,512]{1,0:T(8,128)(2,1)S(1)} %shard_map.82) | data formatting | bytes 524288
